TPU v7x, 32 devices: a whole 2x2x4 slice. The times are simulated.
32 devices in a mesh: grp: 2 (over y), fs: 4 (over z), tp: 4 (over x, core).
Axes of the slice: x: 2, y: 2, z: 4, core: 2. Of those that a mesh axis runs over, the one named last changes fastest.
Arguments:
- tokens: bfloat16 [4096, 2048], P(('grp', 'fs')), parts along dimension 0, may hold values from -6 to 6
- pre_gain: float32 [2048], replicated, may hold values from 0.1 to 1.9
- gate_weight: float32 [2048, 5632], P('fs', 'tp'), may hold values from -0.125 to 0.125
- gate_scale: float32 [5632], P('tp'), may hold values from 0.5 to 2
- up_weight: float32 [2048, 5632], P('fs', 'tp'), may hold values from -0.125 to 0.125
- up_scale: float32 [5632], P('tp'), may hold values from 0.5 to 2
- down_weight: float32 [5632, 2048], P('tp', 'fs'), may hold values from -0.078125 to 0.078125
- down_scale: float32 [2048], replicated, may hold values from 0.3 to 3
- post_gain: float32 [2048], replicated, may hold values from 0.1 to 1.9
Outputs:
- mixed: bfloat16 [4096, 2048], P(('grp', 'fs')), parts along dimension 0
There are 2 independent parts, one for each index of `grp`. A program takes and returns all parts, laid end to end along the dimension named above; an argument that names none is the same for every part. Nothing has to cross between parts.
All inputs are finite; a program needn't handle non-finite values.
Results may differ from a plain program's by a relative error of at most 0.018.
Values may be sent and summed in bfloat16 or wider, within the bound.
A program may use at most 64 MiB of HBM per device.

v0:
```python
import jax
import jax.numpy as jnp
from jax import lax
from jax.sharding import PartitionSpec as P

EPS = 1e-06


def finish(summed, down_scale, post_gain):
    branch = summed * down_scale
    return (
        branch * lax.rsqrt(jnp.mean(branch * branch, axis=-1, keepdims=True) + EPS) * post_gain
    ).astype(jnp.bfloat16)


def body(
    tokens,
    pre_gain,
    gate_weight,
    gate_scale,
    up_weight,
    up_scale,
    down_weight,
    down_scale,
    post_gain,
):
    rows = tokens.astype(jnp.float32)
    normed = (
        rows * lax.rsqrt(jnp.mean(rows * rows, axis=-1, keepdims=True) + EPS) * pre_gain
    ).astype(jnp.bfloat16)
    gate_low = gate_weight.astype(jnp.bfloat16)
    up_low = up_weight.astype(jnp.bfloat16)
    down_low = down_weight.astype(jnp.bfloat16)
    gate_full, up_full = (
        lax.all_gather(gate_low, "fs", axis=0, tiled=True),
        lax.all_gather(up_low, "fs", axis=0, tiled=True),
    )
    gate = jnp.dot(normed, gate_full, preferred_element_type=jnp.float32) * gate_scale
    up = jnp.dot(normed, up_full, preferred_element_type=jnp.float32) * up_scale
    hidden = (jax.nn.silu(gate) * up).astype(jnp.bfloat16)
    down_full = lax.all_gather(down_low, "fs", axis=1, tiled=True)
    partial_value = jnp.dot(hidden, down_full, preferred_element_type=jnp.float32)
    summed = lax.psum(partial_value.astype(jnp.bfloat16), "tp").astype(jnp.float32)
    return finish(summed, down_scale, post_gain)


def solution(mesh):
    in_specs = (
        P(("grp", "fs"), None),
        P(),
        P("fs", "tp"),
        P("tp"),
        P("fs", "tp"),
        P("tp"),
        P("tp", "fs"),
        P(),
        P(),
    )
    out_specs = P(("grp", "fs"), None)
    return jax.shard_map(body, mesh=mesh, in_specs=in_specs, out_specs=out_specs, check_vma=False)
```

profile of v0, /device:TPU:0, one launch (start us, length us, event | category | flops | bytes accessed | tf_op | source)
XLA Modules:
  0.0 406.5 jit_solution(4546783857032367066)
XLA Ops:
  6.5 0.0 copy-start.1
  6.5 0.0 all-gather.4.cloned.1.call-start
  6.5 3.2 convert_element_type.29
  9.8 0.0 all-gather.4.cloned.1.call-update
  9.8 0.0 all-gather.6.cloned.1.call-start
  9.9 0.0 copy-done.1
  9.9 1.3 convert_element_type.30
  11.1 0.0 all-gather.6.cloned.1.call-update
  11.2 0.0 copy-start.2
  11.2 0.0 copy-start.5
  11.2 0.0 copy-start.6
  11.2 0.0 all-gather.8.cloned.1.call-start
  11.2 3.2 convert_element_type.32
  14.5 0.0 all-gather.8.cloned.1.call-update
  14.5 0.0 all-reduce.2.cloned.1.call-start
  14.5 0.0 copy-done.2
  14.6 0.5 fusion
  15.0 0.0 copy-start.7
  15.1 104.3 %all-gather.4.cloned.1.call-done = bf16[2048,1408]{1,0:T(8,128)(2,1)} async-done(((bf16[512,1408]{1,0:T(8,128)(2,1)}), bf16[2048,1408]{1,0:T(8,128)(2,1)}) %all-gather.4.cloned.1.call-update) | async-done | bytes 5767184 | tf_op jit(solution)/shard_map/all_gather | solution.py:35
  119.4 0.0 copy-done.5
  119.4 0.0 copy-done.6
  119.4 7.6 %convolution_multiply_fusion.1 = f32[512,1408]{1,0:T(8,128)} fusion(bf16[2048,1408]{1,0:T(8,128)(2,1)} %all-gather.4.cloned.1.call-done, f32[1408]{0:T(1024)S(1)} %copy-done.5, bf16[512,2048]{1,0:T(8,128)(2,1)S(1)} %copy-done.2, f32[2048]{0:T(1024)S(1)} %copy-done.6, f32[512]{0:T(512)S(1)} %add_rsqrt_fusion.1), kind=kOutput, calls=%fused_computation.10 | convolution fusion | flops 2957705216 | bytes 10763776 | tf_op jit(solution)/shard_map/dot_general | solution.py:38
  127.0 0.0 copy-start.3
  127.0 98.9 %all-gather.6.cloned.1.call-done = bf16[2048,1408]{1,0:T(8,128)(2,1)} async-done(((bf16[512,1408]{1,0:T(8,128)(2,1)}), bf16[2048,1408]{1,0:T(8,128)(2,1)}) %all-gather.6.cloned.1.call-update) | async-done | bytes 5767184 | tf_op jit(solution)/shard_map/all_gather | solution.py:36
  225.9 106.5 %all-gather.8.cloned.1.call-done = bf16[1408,2048]{1,0:T(8,128)(2,1)} async-done(((bf16[1408,512]{1,0:T(8,128)(2,1)}), bf16[1408,2048]{1,0:T(8,128)(2,1)}) %all-gather.8.cloned.1.call-update) | async-done | bytes 5767184 | tf_op jit(solution)/shard_map/all_gather | solution.py:41
  332.5 0.0 copy-done.7
  332.5 13.3 %convolution_convert_fusion = bf16[512,2048]{1,0:T(8,128)(2,1)} fusion(bf16[1408,2048]{1,0:T(8,128)(2,1)} %all-gather.8.cloned.1.call-done, bf16[2048,1408]{1,0:T(8,128)(2,1)} %all-gather.6.cloned.1.call-done, f32[512,1408]{1,0:T(8,128)} %convolution_multiply_fusion.1, f32[1408]{0:T(1024)S(1)} %copy-done.7, bf16[512,2048]{1,0:T(8,128)(2,1)S(1)} %copy-done.2, ...), kind=kOutput, calls=%fused_computation.12 | convolution fusion | flops 5915869184 | bytes 18628096 | tf_op jit(solution)/shard_map/dot_general | solution.py:42
  345.8 0.0 copy-start.4
  345.8 0.0 all-reduce.2.cloned.1.call-update
  345.8 49.8 %all-reduce.2.cloned.1.call-done = bf16[512,2048]{1,0:T(8,128)(2,1)} async-done(((bf16[512,2048]{1,0:T(8,128)(2,1)}), bf16[512,2048]{1,0:T(8,128)(2,1)}) %all-reduce.2.cloned.1.call-update) | async-done | bytes 2097168 | tf_op jit(solution)/shard_map/psum | solution.py:43
  395.6 0.0 copy-done.3
  395.6 0.0 copy-start
  395.6 2.4 multiply_reduce_fusion
  398.0 0.0 copy-done.4
  398.0 0.0 copy-done
  398.0 2.0 multiply_convert_fusion
  (2 shorter events, 0.0 us)
Async XLA Ops:
  6.5 3.3 copy-start.1
  6.5 112.8 %all-gather.4.cloned.1.call-start = ((), (), s32[]{:S(2)}) async-start(), calls=%async_computation | async-start | bytes 7208960 | tf_op jit(solution)/shard_map/all_gather | solution.py:35
  9.8 216.1 %all-gather.6.cloned.1.call-start = ((), (), s32[]{:S(2)}) async-start(), calls=%async_computation.1 | async-start | bytes 7208960 | tf_op jit(solution)/shard_map/all_gather | solution.py:36
  11.2 3.4 copy-start.2
  11.2 108.2 %copy-start.5 = (f32[1408]{0:T(1024)S(1)}, f32[1408]{0:T(1024)}, u32[]{:S(2)}) copy-start(f32[1408]{0:T(1024)} %param.12) | copy-start | bytes 16900
  11.2 108.2 %copy-start.6 = (f32[2048]{0:T(1024)S(1)}, f32[2048]{0:T(1024)}, u32[]{:S(2)}) copy-start(f32[2048]{0:T(1024)} %param.10) | copy-start | bytes 24580
  11.2 321.3 %all-gather.8.cloned.1.call-start = ((), (), s32[]{:S(2)}) async-start(), calls=%async_computation.2 | async-start | bytes 7208960 | tf_op jit(solution)/shard_map/all_gather | solution.py:41
  14.5 381.1 %all-reduce.2.cloned.1.call-start = ((), (), s32[]{:S(2)}) async-start(), calls=%async_computation.3 | async-start | bytes 4194304 | tf_op jit(solution)/shard_map/psum | solution.py:43
  15.0 317.4 %copy-start.7 = (f32[1408]{0:T(1024)S(1)}, f32[1408]{0:T(1024)}, u32[]{:S(2)}) copy-start(f32[1408]{0:T(1024)} %param.14) | copy-start | bytes 16900
  127.0 268.6 %copy-start.3 = (f32[2048]{0:T(1024)S(1)}, f32[2048]{0:T(1024)}, u32[]{:S(2)}) copy-start(f32[2048]{0:T(1024)} %param.16) | copy-start | bytes 24580
  345.8 52.2 %copy-start.4 = (f32[2048]{0:T(1024)S(1)}, f32[2048]{0:T(1024)}, u32[]{:S(2)}) copy-start(f32[2048]{0:T(1024)} %param.17) | copy-start | bytes 24580
  395.6 2.4 copy-start
Sparse Core Ops, SparseCore 0:
  9.9 109.3 all-gather.3
  120.9 104.9 all-gather.5
  227.5 104.9 all-gather.7
  345.9 49.6 all-reduce.1
where the time goes:
time: 407 us; the launch traced here: 406 us
  waiting for transfers between devices  360 us (88%)
  matrix products  21 us (5%)
  between operations  13.2 us (3%)
  other arithmetic  12.6 us (3%)
    all_gather x1, waiting for transfers between devices, body(): down_full = lax.all_gather(down_low, 'fs', axis=1, tiled=True)  107 us
    all_gather x1, waiting for transfers between devices, body(): lax.all_gather(gate_low, 'fs', axis=0, tiled=True)  104 us
    all_gather x1, waiting for transfers between devices, body(): lax.all_gather(up_low, 'fs', axis=0, tiled=True)  98.9 us
    psum x1, waiting for transfers between devices, body(): lax.psum(partial_value.astype(jnp.bfloat16), 'tp').astype(jnp.float32)  49.8 us
    dot_general x1, matrix products, body(): jnp.dot(hidden, down_full, preferred_element_type=jnp.float32)  13.3 us
  transfers between devices with their start and end apart: 4, of which 4 were waited for; matrix products, arithmetic and copies ran while one was open for 3% of the time, Pallas kernels for 0%

commit v1 on v0

--- a/solution.py
+++ b/solution.py
@@ -11,6 +11,20 @@
     return (
         branch * lax.rsqrt(jnp.mean(branch * branch, axis=-1, keepdims=True) + EPS) * post_gain
     ).astype(jnp.bfloat16)
+
+
+def gather_shards(block):
+    groups, shards = lax.axis_size("grp"), lax.axis_size("fs")
+    rows, columns = block.shape
+    pieces = block.reshape(groups, rows // groups, columns)
+    mine = lax.dynamic_index_in_dim(pieces, lax.axis_index("grp"), 0, keepdims=False)
+    whole = lax.all_gather(mine, ("fs", "grp"), axis=0, tiled=True)
+    return whole.reshape(shards, rows, columns)
+
+
+def gather_shared(block):
+    whole = gather_shards(block)
+    return whole.reshape(-1, block.shape[1])
 
 
 def body(
@@ -31,15 +45,14 @@
     gate_low = gate_weight.astype(jnp.bfloat16)
     up_low = up_weight.astype(jnp.bfloat16)
     down_low = down_weight.astype(jnp.bfloat16)
-    gate_full, up_full = (
-        lax.all_gather(gate_low, "fs", axis=0, tiled=True),
-        lax.all_gather(up_low, "fs", axis=0, tiled=True),
-    )
+    gate_full, up_full = gather_shared(gate_low), gather_shared(up_low)
     gate = jnp.dot(normed, gate_full, preferred_element_type=jnp.float32) * gate_scale
     up = jnp.dot(normed, up_full, preferred_element_type=jnp.float32) * up_scale
     hidden = (jax.nn.silu(gate) * up).astype(jnp.bfloat16)
-    down_full = lax.all_gather(down_low, "fs", axis=1, tiled=True)
-    partial_value = jnp.dot(hidden, down_full, preferred_element_type=jnp.float32)
+    shards = gather_shards(down_low)
+    partial_value = jnp.concatenate(
+        [jnp.dot(hidden, shards[k], preferred_element_type=jnp.float32) for k in range(shards.shape[0])], axis=1
+    )
     summed = lax.psum(partial_value.astype(jnp.bfloat16), "tp").astype(jnp.float32)
     return finish(summed, down_scale, post_gain)
 

time: 407 us -> 361 us (0.89)
  waiting for transfers between devices: 360 us -> 309 us
  local copies, waits for them, and re-layouts: 0.04 us -> 6.02 us
    all_gather x3, waiting for transfers between devices: 310 us -> 259 us  [gather_shards(): whole = lax.all_gather(mine, ('fs', 'grp'), axis=0, tiled=True)]
    dot_general x1 -> x5, matrix products: 13.3 us -> 15.2 us  [the longest x1 7.8 us: body(): up = jnp.dot(normed, up_full, preferred_element_type=jnp.float32) * up_scale]
  transfers between devices with their start and end apart: 4 -> 4, of which waited for: 4 -> 4; matrix products, arithmetic and copies ran while one was open for 3% -> 6% of each run, Pallas kernels for 0% -> 0%
where the time goes in v1:
time: 361 us
  waiting for transfers between devices  309 us (86%)
  matrix products  22.9 us (6%)
  between operations  13.3 us (4%)
  other arithmetic  9.44 us (3%)
  local copies, waits for them, and re-layouts  6.02 us (2%)
    all_gather x3, waiting for transfers between devices, gather_shards(): whole = lax.all_gather(mine, ('fs', 'grp'), axis=0, tiled=True)  259 us
    psum x1, waiting for transfers between devices, body(): lax.psum(partial_value.astype(jnp.bfloat16), 'tp').astype(jnp.float32)  49.7 us
    dot_general x1, matrix products, body(): up = jnp.dot(normed, up_full, preferred_element_type=jnp.float32) * up_scale  7.8 us
    dot_general x1, matrix products, body(): jnp.dot(normed, gate_full, preferred_element_type=jnp.float32) * gate_scale  7.64 us
    dot_general x4, matrix products, body(): jnp.dot(hidden, shards[k], preferred_element_type=jnp.float32)  7.42 us
  transfers between devices with their start and end apart: 4, of which 4 were waited for; matrix products, arithmetic and copies ran while one was open for 6% of the time, Pallas kernels for 0%

profile of v1, /device:TPU:0, one launch (start us, length us, event | category | flops | bytes accessed | tf_op | source)
XLA Modules:
  0.0 360.9 jit_solution(10505173811535307966)
XLA Ops:
  6.5 0.0 all-gather.7.cloned.1.call-start
  6.5 2.0 convert_element_type.27
  8.5 0.9 constant_dynamic-slice_fusion.2
  9.4 0.0 all-gather.7.cloned.1.call-update
  9.5 0.0 copy-start.1
  9.5 0.0 all-gather.9.cloned.1.call-start
  9.5 2.1 convert_element_type.28
  11.6 0.9 constant_dynamic-slice_fusion.1
  12.6 0.0 all-gather.9.cloned.1.call-update
  12.6 0.0 all-gather.11.cloned.1.call-start
  12.6 0.0 copy-done.1
  12.6 0.2 convert_element_type.30
  12.8 0.0 copy-start.2
  12.8 0.0 copy-start.6
  12.9 0.0 copy-start.7
  12.9 0.9 constant_dynamic-slice_fusion
  13.8 0.0 all-gather.11.cloned.1.call-update
  13.8 0.0 all-reduce.2.cloned.1.call-start
  13.9 0.8 copy-done.2
  14.7 0.5 fusion.4
  15.2 0.0 copy-start.8
  15.2 89.5 %all-gather.7.cloned.1.call-done = bf16[1,2048,1408]{2,1,0:T(8,128)(2,1)} async-done(((bf16[1,256,1408]{2,1,0:T(8,128)(2,1)}), bf16[1,2048,1408]{2,1,0:T(8,128)(2,1)}) %all-gather.7.cloned.1.call-update) | async-done | bytes 5767184 | tf_op jit(solution)/shard_map/all_gather | solution.py:21
  104.6 0.0 copy-done.6
  104.6 0.0 copy-done.7
  104.6 7.6 %fusion.7 = f32[512,1408]{1,0:T(8,128)} fusion(bf16[1,2048,1408]{2,1,0:T(8,128)(2,1)} %all-gather.7.cloned.1.call-done, f32[1408]{0:T(1024)S(1)} %copy-done.6, bf16[512,2048]{1,0:T(8,128)(2,1)S(1)} %copy-done.2, f32[2048]{0:T(1024)S(1)} %copy-done.7, f32[512]{0:T(512)S(1)} %add_rsqrt_fusion.1), kind=kOutput, calls=%fused_computation.12 | convolution fusion | flops 2957705216 | bytes 10763776 | tf_op jit(solution)/shard_map/dot_general | solution.py:49
  112.3 85.1 %all-gather.9.cloned.1.call-done = bf16[1,2048,1408]{2,1,0:T(8,128)(2,1)} async-done(((bf16[1,256,1408]{2,1,0:T(8,128)(2,1)}), bf16[1,2048,1408]{2,1,0:T(8,128)(2,1)}) %all-gather.9.cloned.1.call-update) | async-done | bytes 5767184 | tf_op jit(solution)/shard_map/all_gather | solution.py:21
  197.3 0.0 copy-done.8
  197.3 7.8 %fusion.16 = bf16[512,1408]{1,0:T(8,128)(2,1)} fusion(bf16[1,2048,1408]{2,1,0:T(8,128)(2,1)} %all-gather.9.cloned.1.call-done, f32[512,1408]{1,0:T(8,128)} %fusion.7, f32[1408]{0:T(1024)S(1)} %copy-done.8, bf16[512,2048]{1,0:T(8,128)(2,1)S(1)} %copy-done.2, f32[2048]{0:T(1024)S(1)} %copy-done.7, f32[512]{0:T(512)S(1)} %add_rsqrt_fusion.1), kind=kOutput, calls=%fused_computation.15 | convolution fusion | flops 2962030592 | bytes 12205568 | tf_op jit(solution)/shard_map/dot_general | solution.py:50
  205.2 0.0 copy-start.9
  205.2 84.9 %all-gather.11.cloned.1.call-done = bf16[1,5632,512]{2,1,0:T(8,128)(2,1)} async-done(((bf16[1,704,512]{2,1,0:T(8,128)(2,1)}), bf16[1,5632,512]{2,1,0:T(8,128)(2,1)}) %all-gather.11.cloned.1.call-update) | async-done | bytes 5767184 | tf_op jit(solution)/shard_map/all_gather | solution.py:21
  290.1 0.0 copy-start.5
  290.1 3.0 fusion.25
  293.0 0.0 copy-done.9
  293.0 2.4 fusion.24
  295.4 0.0 copy-done.5
  295.5 1.0 fusion.23
  296.5 1.0 fusion.26
  297.5 0.0 copy-start.3
  297.5 1.5 pad_maximum_fusion
  299.0 0.0 copy-start.4
  299.0 0.0 all-reduce.2.cloned.1.call-update
  299.0 49.7 %all-reduce.2.cloned.1.call-done = bf16[512,2048]{0,1:T(8,128)(2,1)} async-done(((bf16[512,2048]{0,1:T(8,128)(2,1)}), bf16[512,2048]{0,1:T(8,128)(2,1)}) %all-reduce.2.cloned.1.call-update) | async-done | bytes 2097168 | tf_op jit(solution)/shard_map/psum | solution.py:56
  348.7 0.0 copy-done.3
  348.7 2.4 multiply_reduce_fusion
  351.1 0.0 copy-done.4
  351.1 0.0 copy-done
  351.1 0.9 multiply_convert_fusion
  352.0 2.4 copy.10
  (3 shorter events, 0.0 us)
Async XLA Ops:
  6.5 98.1 %all-gather.7.cloned.1.call-start = ((), (), s32[]{:S(2)}) async-start(), calls=%async_computation.1 | async-start | bytes 6488064 | tf_op jit(solution)/shard_map/all_gather | solution.py:21
  9.5 3.2 copy-start.1
  9.5 187.9 %all-gather.9.cloned.1.call-start = ((), (), s32[]{:S(2)}) async-start(), calls=%async_computation.2 | async-start | bytes 6488064 | tf_op jit(solution)/shard_map/all_gather | solution.py:21
  12.6 277.5 %all-gather.11.cloned.1.call-start = ((), (), s32[]{:S(2)}) async-start(), calls=%async_computation.3 | async-start | bytes 6488064 | tf_op jit(solution)/shard_map/all_gather | solution.py:21
  12.8 1.9 copy-start.2
  12.8 91.8 %copy-start.6 = (f32[1408]{0:T(1024)S(1)}, f32[1408]{0:T(1024)}, u32[]{:S(2)}) copy-start(f32[1408]{0:T(1024)} %param.12) | copy-start | bytes 16900
  12.9 91.8 %copy-start.7 = (f32[2048]{0:T(1024)S(1)}, f32[2048]{0:T(1024)}, u32[]{:S(2)}) copy-start(f32[2048]{0:T(1024)} %param.10) | copy-start | bytes 24580
  13.8 334.9 %all-reduce.2.cloned.1.call-start = ((), (), s32[]{:S(2)}) async-start(), calls=%async_computation | async-start | bytes 4194304 | tf_op jit(solution)/shard_map/psum | solution.py:56
  15.2 182.2 %copy-start.8 = (f32[1408]{0:T(1024)S(1)}, f32[1408]{0:T(1024)}, u32[]{:S(2)}) copy-start(f32[1408]{0:T(1024)} %param.14) | copy-start | bytes 16900
  205.2 87.9 %copy-start.9 = (bf16[512,1408]{1,0:T(8,128)(2,1)S(1)}, bf16[512,1408]{1,0:T(8,128)(2,1)}, u32[]{:S(2)}) copy-start(bf16[512,1408]{1,0:T(8,128)(2,1)} %fusion.16) | copy-start | bytes 4325380
  290.1 5.4 %copy-start.5 = (bf16[1,5632,512]{2,1,0:T(8,128)(2,1)S(1)}, bf16[1,5632,512]{2,1,0:T(8,128)(2,1)}, u32[]{:S(2)}) copy-start(bf16[1,5632,512]{2,1,0:T(8,128)(2,1)} %all-gather.11.cloned.1.call-done) | copy-start | bytes 17301508
  297.5 51.2 %copy-start.3 = (f32[2048]{0:T(1024)S(1)}, f32[2048]{0:T(1024)}, u32[]{:S(2)}) copy-start(f32[2048]{0:T(1024)} %param.16) | copy-start | bytes 24580
  299.0 52.1 %copy-start.4 = (f32[2048]{0:T(1024)S(1)}, f32[2048]{0:T(1024)}, u32[]{:S(2)}) copy-start(f32[2048]{0:T(1024)} %param.17) | copy-start | bytes 24580
  348.7 2.4 copy-start
Sparse Core Ops, SparseCore 0:
  9.6 95.0 all-gather.6
  106.8 90.4 all-gather.8
  199.5 90.4 all-gather.10
  299.1 49.5 all-reduce.1

commit v2 on v1

--- a/solution.py
+++ b/solution.py
@@ -1,9 +1,284 @@
+import functools
+
 import jax
 import jax.numpy as jnp
 from jax import lax
+from jax.experimental import pallas as pl
+from jax.experimental.pallas import tpu as pltpu
 from jax.sharding import PartitionSpec as P
 
 EPS = 1e-06
+LANES = 128
+ORDER = (0, 1, 3, 2)
+
+
+def up_to(value, step):
+    return -(-value // step) * step
+
+
+def fused(
+    sizes, pieces_ref, token_ref, scale_ref, gain_ref, out_ref,
+    held, toks, acc, hid, part, red,
+    own_sem, got, sent_z, sent_x, sent_y, sent_s,
+    tok_own, tok_got, tok_sent, red_got, red_sent, out_got, out_sent,
+):
+    unit, block, half, width = sizes
+    n_y, n_z, n_t = held.shape[:3]
+    y, z, t = lax.axis_index("grp"), lax.axis_index("fs"), lax.axis_index("tp")
+    x, c = t // 2, t % 2
+    t_x, t_s, t_d = (1 - x) * 2 + c, x * 2 + 1 - c, (1 - x) * 2 + 1 - c
+    y_o = 1 - y
+    xn, yn, sn = {"tp": t_x}, {"grp": y_o}, {"tp": t_s}
+
+    barrier = pltpu.get_barrier_semaphore()
+    peers = [{"fs": (z + d) % n_z} for d in range(1, n_z)] + [xn, yn, sn]
+    for peer in peers:
+        pl.semaphore_signal(barrier, inc=1, device_id=peer, device_id_type=pl.DeviceIdType.MESH)
+    pl.semaphore_wait(barrier, len(peers))
+
+    pending = []
+
+    def send(src, dst, s_sem, r_sem, to):
+        copy = pltpu.make_async_remote_copy(
+            src_ref=src, dst_ref=dst, send_sem=s_sem, recv_sem=r_sem,
+            device_id=to, device_id_type=pl.DeviceIdType.MESH,
+        )
+        copy.start()
+        return copy
+
+    def pass_on(slot, sems, to):
+        pending.append(send(held.at[slot], held.at[slot], sems.at[slot], got.at[slot], to))
+
+    def arrived(slot):
+        pltpu.make_async_remote_copy(
+            src_ref=held.at[slot], dst_ref=held.at[slot], send_sem=sent_s.at[slot], recv_sem=got.at[slot],
+            device_id=sn, device_id_type=pl.DeviceIdType.MESH,
+        ).wait_recv()
+
+    own = pltpu.make_async_copy(pieces_ref.at[z], held.at[y, z, t], own_sem)
+    own.start()
+    own_tok = pltpu.make_async_copy(token_ref, toks.at[z], tok_own)
+    own_tok.start()
+
+    def send_piece(d):
+        to = (z + d) % n_z
+        pending.append(send(pieces_ref.at[to], held.at[y, z, t], sent_z.at[d], got.at[y, z, t], {"fs": to}))
+
+    def token_copy(src, slot, side):
+        return pltpu.make_async_remote_copy(
+            src_ref=src, dst_ref=toks.at[slot], send_sem=tok_sent.at[slot, side], recv_sem=tok_got.at[slot],
+            device_id={"fs": (z + 1 if side else z - 1 + n_z) % n_z}, device_id_type=pl.DeviceIdType.MESH,
+        )
+
+    send_piece(ORDER[1])
+    for side in (0, 1):
+        @pl.when((z < n_z - 1) if side else (z > 0))
+        def _():
+            token_copy(token_ref, z, side).start()
+    for d in ORDER[2:]:
+        send_piece(d)
+
+    def zs_of(i):
+        return (z - ORDER[i] + n_z) % n_z
+
+    def first(i):
+        slot = (y, zs_of(i), t)
+        if i == 0:
+            own.wait()
+        else:
+            arrived(slot)
+        pass_on(slot, sent_x, xn)
+        pass_on(slot, sent_y, yn)
+        pass_on(slot, sent_s, sn)
+
+    def second(i):
+        zs = zs_of(i)
+        slot = (y, zs, t_x)
+        arrived(slot)
+        if i % 2 == 0:
+            pass_on(slot, sent_y, yn)
+        pass_on(slot, sent_s, sn)
+        slot = (y_o, zs, t)
+        arrived(slot)
+        if i % 2 == 1:
+            pass_on(slot, sent_x, xn)
+        pass_on(slot, sent_s, sn)
+
+    def third(i):
+        slot = (y_o, zs_of(i), t_x)
+        arrived(slot)
+        pass_on(slot, sent_s, sn)
+
+    def siblings(i):
+        zs = zs_of(i)
+        for q, tt in ((y, t_s), (y, t_d), (y_o, t_s), (y_o, t_d)):
+            arrived((q, zs, tt))
+
+    def multiply(i):
+        zs = zs_of(i)
+
+        @pl.loop(0, n_t)
+        def _(tt):
+            for q in range(n_y):
+                columns = pl.ds(pl.multiple_of((zs * n_y + q) * half, half), half)
+                rows = toks[:, :, columns].reshape(-1, half)
+                weight = jnp.concatenate(
+                    [held[q, zs, tt, pl.ds(k * half, half), :] for k in range(2 * block // LANES)], axis=1
+                )
+                value = jnp.dot(rows, weight, preferred_element_type=jnp.float32)
+                if i == 0 and q == 0:
+                    acc[tt] = value
+                else:
+                    acc[tt] += value
+
+    def tokens_on():
+        for k in range(1, n_z):
+            for side in (0, 1):
+                here = (z - k >= 0) if side else (z + k < n_z)
+
+                @pl.when(here)
+                def _():
+                    slot = (z - k if side else z + k) % n_z
+                    token_copy(toks.at[slot], slot, side).wait_recv()
+
+                    @pl.when((z + 1 < n_z) if side else (z > 0))
+                    def _():
+                        token_copy(toks.at[slot], slot, side).start()
+
+    first(0)
+    own_tok.wait()
+    first(1)
+    second(0)
+    tokens_on()
+    first(2)
+    third(0)
+    second(1)
+    siblings(0)
+    multiply(0)
+    first(3)
+    third(1)
+    second(2)
+    siblings(1)
+    multiply(1)
+    second(3)
+    third(2)
+    siblings(2)
+    multiply(2)
+    third(3)
+    siblings(3)
+    multiply(3)
+
+    @pl.loop(0, n_t)
+    def _(tt):
+        gate, up = acc[tt, :, :block], acc[tt, :, block:]
+        hid[tt] = (gate / (1.0 + jnp.exp(-gate)) * up).astype(jnp.bfloat16)[:, :unit]
+
+    base = 2 * block // LANES * half
+    fan = half // LANES
+    red_sends = []
+    for zs in range(n_z):
+        for q in range(n_y):
+            total = None
+            for tt in range(n_t):
+                weight = jnp.concatenate(
+                    [held[q, zs, tt, pl.ds(base + k * unit, unit), :] for k in range(fan)], axis=1
+                )
+                value = jnp.dot(hid[tt], weight, preferred_element_type=jnp.float32)
+                total = value if total is None else total + value
+            part[:, :, pl.ds((zs * n_y + q) * half, half)] = total.astype(jnp.bfloat16).reshape(n_z, -1, half)
+        columns = pl.ds(zs * n_y * half, n_y * half)
+        for d in ORDER[1:]:
+            to = (z + d) % n_z
+            red_sends.append(send(
+                part.at[to, :, columns], red.at[d, :, columns],
+                red_sent.at[d, zs], red_got.at[d, zs], {"fs": to},
+            ))
+    for copy in red_sends:
+        copy.wait_recv()
+    summed = part[z].astype(jnp.float32)
+    for d in range(1, n_z):
+        summed += red[d].astype(jnp.float32)
+    branch = summed * scale_ref[...]
+    mean = jnp.mean(branch * branch, axis=-1, keepdims=True)
+    out_ref[t] = (branch * lax.rsqrt(mean + EPS) * gain_ref[...]).astype(jnp.bfloat16)
+
+    def give(slot, k, to):
+        pending.append(send(out_ref.at[slot], out_ref.at[slot], out_sent.at[k], out_got.at[slot], to))
+
+    def taken(slot):
+        pltpu.make_async_remote_copy(
+            src_ref=out_ref.at[slot], dst_ref=out_ref.at[slot], send_sem=out_sent.at[0], recv_sem=out_got.at[slot],
+            device_id=sn, device_id_type=pl.DeviceIdType.MESH,
+        ).wait_recv()
+
+    give(t, 0, xn)
+    give(t, 1, sn)
+    taken(t_x)
+    give(t_x, 2, sn)
+    taken(t_s)
+    taken(t_d)
+    for copy in pending + red_sends:
+        copy.wait_send()
+    for side in (0, 1):
+        for k in range(0, n_z):
+            origin = (z - k >= 0) if side else (z + k < n_z)
+
+            @pl.when(origin & ((z + 1 < n_z) if side else (z > 0)))
+            def _():
+                slot = (z - k if side else z + k) % n_z
+                token_copy(toks.at[slot], slot, side).wait_send()
+
+
+def quad_body(
+    tokens, pre_gain, gate_weight, gate_scale, up_weight, up_scale, down_weight, down_scale, post_gain,
+):
+    n_y, n_z, n_t = (lax.axis_size(a) for a in ("grp", "fs", "tp"))
+    y, t = lax.axis_index("grp"), lax.axis_index("tp")
+    shard, hidden = gate_weight.shape
+    unit, half = hidden // n_z, shard // n_y
+    block = up_to(unit, LANES)
+    share, width = tokens.shape[0] // n_t, tokens.shape[1]
+
+    rows = lax.dynamic_slice_in_dim(tokens, t * share, share, 0).astype(jnp.float32)
+    normed = (
+        rows * lax.rsqrt(jnp.mean(rows * rows, axis=-1, keepdims=True) + EPS) * pre_gain
+    ).astype(jnp.bfloat16)
+
+    def pieces_of(weight, scale):
+        mine = lax.dynamic_slice_in_dim(weight, y * half, half, 0)
+        low = (mine * scale).astype(jnp.bfloat16).reshape(half, n_z, unit)
+        low = jnp.pad(low, ((0, 0), (0, 0), (0, block - unit)))
+        return low.reshape(half, n_z, block // LANES, LANES).transpose(1, 2, 0, 3).reshape(n_z, -1, LANES)
+
+    mine = lax.dynamic_slice_in_dim(down_weight, y * half, half, 1).astype(jnp.bfloat16)
+    low = mine.reshape(n_z, unit, half // LANES, LANES).transpose(0, 2, 1, 3).reshape(n_z, -1, LANES)
+    pieces = jnp.concatenate(
+        [pieces_of(gate_weight, gate_scale), pieces_of(up_weight, up_scale), low], axis=1
+    )
+    depth = pieces.shape[1]
+    bf16, f32, dma = jnp.bfloat16, jnp.float32, pltpu.SemaphoreType.DMA
+    slots = (n_y, n_z, n_t)
+    vmem = pl.BlockSpec(memory_space=pltpu.VMEM)
+    out = pl.pallas_call(
+        functools.partial(fused, (unit, block, half, width)),
+        out_shape=jax.ShapeDtypeStruct((n_t, share, width), bf16),
+        in_specs=[vmem] * 4,
+        out_specs=vmem,
+        scratch_shapes=[
+            pltpu.VMEM(slots + (depth, LANES), bf16),
+            pltpu.VMEM((n_z, share, width), bf16),
+            pltpu.VMEM((n_t, n_z * share, 2 * block), f32),
+            pltpu.VMEM((n_t, n_z * share, unit), bf16),
+            pltpu.VMEM((n_z, share, width), bf16),
+            pltpu.VMEM((n_z, share, width), bf16),
+            dma, dma(slots), dma((n_z,)), dma(slots), dma(slots), dma(slots),
+            dma, dma((n_z,)), dma((n_z, 2)), dma((n_z, n_z)), dma((n_z, n_z)), dma((n_t,)), dma((3,)),
+        ],
+        compiler_params=pltpu.CompilerParams(
+            collective_id=0, has_side_effects=True, vmem_limit_bytes=60 * 2**20
+        ),
+    )(pieces, normed, down_scale[None], post_gain[None])
+    return out.reshape(n_t * share, width)
 
 
 def finish(summed, down_scale, post_gain):
@@ -70,4 +345,6 @@
         P(),
     )
     out_specs = P(("grp", "fs"), None)
-    return jax.shard_map(body, mesh=mesh, in_specs=in_specs, out_specs=out_specs, check_vma=False)
+    sizes = tuple(mesh.shape[a] for a in ("grp", "fs", "tp"))
+    chosen = quad_body if sizes == (2, 4, 4) else body
+    return jax.shard_map(chosen, mesh=mesh, in_specs=in_specs, out_specs=out_specs, check_vma=False)

time: 361 us -> 233 us (0.65)
  waiting for transfers between devices: 309 us -> 0 us
  Pallas kernels: 0 us -> 197 us
  matrix products: 22.9 us -> 0 us
  local copies, waits for them, and re-layouts: 6.02 us -> 24 us
  between operations: 13.3 us -> 0.05 us
    all_gather x3 -> x0, waiting for transfers between devices: 259 us -> none  [gather_shards(): whole = lax.all_gather(mine, ('fs', 'grp'), axis=0, tiled=True)]
    pallas_call x0 -> x1, Pallas kernels: none -> 197 us  [quad_body(): pl.pallas_call(functools.partial(fused, (unit, block, half, width)), out_...]
    psum x1 -> x0, waiting for transfers between devices: 49.7 us -> none  [body(): lax.psum(partial_value.astype(jnp.bfloat16), 'tp').astype(jnp.float32)]
    dot_general x6 -> x0, matrix products: 22.9 us -> none  [the longest x1 7.8 us: body(): up = jnp.dot(normed, up_full, preferred_element_type=jnp.float32) * up_scale]
    unnamed x20 -> x11, local copies, waits for them, and re-layouts: 0.86 us -> 9.03 us
    transpose x0 -> x2, local copies, waits for them, and re-layouts: none -> 4.61 us  [pieces_of(): low.reshape(half, n_z, block // LANES, LANES).transpose(1, 2, 0, 3)]
    reshape x0 -> x2, local copies, waits for them, and re-layouts: none -> 3.81 us  [quad_body(): mine.reshape(n_z, unit, half // LANES, LANES).transpose(0, 2, 1, 3)]
  transfers between devices with their start and end apart: 4 -> 0, of which waited for: 4 -> 0; matrix products, arithmetic and copies ran while one was open for 6% -> 0% of each run, Pallas kernels for 0% -> 0%
where the time goes in v2:
time: 233 us; the launch traced here: 231 us
  Pallas kernels  197 us (85%)
  local copies, waits for them, and re-layouts  24 us (10%)
  other arithmetic  9.41 us (4%)
    pallas_call x1, Pallas kernels, quad_body(): pl.pallas_call(functools.partial(fused, (unit, block, half, width)), out_...  197 us
    unnamed x11, local copies, waits for them, and re-layouts  9.03 us

profile of v2, /device:TPU:0, one launch (start us, length us, event | category | flops | bytes accessed | tf_op | source)
XLA Modules:
  0.0 230.8 jit_solution(6833111718313297460)
XLA Ops:
  0.0 0.0 copy-start
  0.0 3.7 %constant_dynamic-slice_fusion = (f32[256,1408]{1,0:T(8,128)}, f32[256,1408]{1,0:T(8,128)}) fusion(f32[512,1408]{1,0:T(8,128)} %param.13, s32[]{:T(128)S(6)} %select_n.8, f32[512,1408]{1,0:T(8,128)} %param.11), kind=kLoop, calls=%fused_computation.9 | loop fusion | bytes 5767172 | tf_op jit(solution)/shard_map/dynamic_slice | solution.py:248
  3.7 0.0 copy-start.1
  3.7 2.9 %copy.16 = f32[256,1408]{0,1:T(8,128)} copy(f32[256,1408]{1,0:T(8,128)} %get-tuple-element.6) | data formatting | bytes 2883584
  6.7 0.0 copy-done.1
  6.7 1.6 multiply_convert_fusion.1
  8.3 0.9 pad.7
  9.2 0.0 copy-start.2
  9.2 2.3 %copy.12 = bf16[4,3,256,128]{3,2,1,0:T(8,128)(2,1)} copy(bf16[4,3,256,128]{2,3,1,0:T(8,128)(2,1)} %bitcast.20) | data formatting | bytes 1572864 | tf_op jit(solution)/shard_map/transpose | solution.py:251
  11.6 2.9 %copy.17 = f32[256,1408]{0,1:T(8,128)} copy(f32[256,1408]{1,0:T(8,128)} %get-tuple-element.5) | data formatting | bytes 2883584
  14.5 0.0 copy-done.2
  14.5 1.6 multiply_convert_fusion
  16.1 0.9 pad.8
  17.1 2.3 copy.14
  19.3 0.0 copy-done
  19.3 1.0 dynamic-slice_convert_fusion
  20.3 2.6 %reshape.44 = bf16[4,352,2,128]{3,2,1,0:T(2,128)(2,1)} reshape(bf16[1408,256]{1,0:T(8,128)(2,1)} %dynamic-slice_convert_fusion) | data formatting | bytes 1441792 | tf_op jit(solution)/shard_map/reshape | solution.py:254
  22.9 1.2 copy.15
  24.1 0.0 copy-start.3
  24.1 2.9 %pad_maximum_fusion.pieces_ref = bf16[4,2240,128]{2,1,0:T(8,128)(2,1)} fusion(bf16[4,704,128]{2,1,0:T(8,128)(2,1)S(1)} %bitcast.21, bf16[4,768,128]{2,1,0:T(8,128)(2,1)} %bitcast.18, bf16[4,768,128]{2,1,0:T(8,128)(2,1)} %bitcast.17), kind=kLoop, calls=%fused_computation | loop fusion | flops 6881280 | bytes 4587520 | tf_op jit(solution)/shard_map/concatenate | solution.py:255
  27.0 1.2 fusion
  28.3 0.0 copy-done.3
  28.3 2.0 fusion.2.token_ref
  30.3 197.3 %shard_map.91 = bf16[4,128,2048]{2,1,0:T(8,128)(2,1)} custom-call(bf16[4,2240,128]{2,1,0:T(8,128)(2,1)} %pad_maximum_fusion.pieces_ref, bf16[128,2048]{1,0:T(8,128)(2,1)} %fusion.2.token_ref, f32[1,2048]{1,0:T(1,128)} %bitcast.24, f32[1,2048]{1,0:T(1,128)} %bitcast.25), custom_call_target="tpu_custom_call" | custom-call | tf_op jit(solution)/shard_map/pallas_call | solution.py:262
  227.6 3.2 %copy.19 = bf16[512,2048]{1,0:T(8,128)(2,1)} copy(bf16[512,2048]{1,0:T(8,128)(2,1)} %bitcast.16) | data formatting | bytes 4194304
  (1 shorter events, 0.0 us)
Async XLA Ops:
  0.0 19.3 %copy-start = (f32[1408,512]{1,0:T(8,128)S(1)}, f32[1408,512]{1,0:T(8,128)}, u32[]{:S(2)}) copy-start(f32[1408,512]{1,0:T(8,128)} %param.15) | copy-start | bytes 8650756
  3.7 2.9 %copy-start.1 = (f32[1408]{0:T(1024)S(1)}, f32[1408]{0:T(1024)}, u32[]{:S(2)}) copy-start(f32[1408]{0:T(1024)} %param.12) | copy-start | bytes 16900
  9.2 5.3 %copy-start.2 = (f32[1408]{0:T(1024)S(1)}, f32[1408]{0:T(1024)}, u32[]{:S(2)}) copy-start(f32[1408]{0:T(1024)} %param.14) | copy-start | bytes 16900
  24.1 4.2 %copy-start.3 = (f32[2048]{0:T(1024)S(1)}, f32[2048]{0:T(1024)}, u32[]{:S(2)}) copy-start(f32[2048]{0:T(1024)} %param.10) | copy-start | bytes 24580

commit v3 on v2

--- a/solution.py
+++ b/solution.py
@@ -17,8 +17,8 @@
 
 
 def fused(
-    sizes, pieces_ref, token_ref, scale_ref, gain_ref, out_ref,
-    held, toks, acc, hid, part, red,
+    sizes, gate_ref, up_ref, down_ref, token_ref, scale_ref, gain_ref, out_ref,
+    pieces_ref, held, toks, acc, hid, part, red,
     own_sem, got, sent_z, sent_x, sent_y, sent_s,
     tok_own, tok_got, tok_sent, red_got, red_sent, out_got, out_sent,
 ):
@@ -34,6 +34,18 @@
     peers = [{"fs": (z + d) % n_z} for d in range(1, n_z)] + [xn, yn, sn]
     for peer in peers:
         pl.semaphore_signal(barrier, inc=1, device_id=peer, device_id_type=pl.DeviceIdType.MESH)
+    for k in range(n_z):
+        for j, ref in enumerate((gate_ref, up_ref)):
+            for b in range(block // LANES):
+                lanes = min(LANES, unit - b * LANES)
+                rows = pl.ds((j * (block // LANES) + b) * half, half)
+                pieces_ref[k, rows, :lanes] = ref[:, k * unit + b * LANES:k * unit + b * LANES + lanes]
+                if lanes < LANES:
+                    pieces_ref[k, rows, lanes:] = jnp.zeros((half, LANES - lanes), jnp.bfloat16)
+        for b in range(half // LANES):
+            pieces_ref[k, pl.ds(2 * block // LANES * half + b * unit, unit), :] = down_ref[
+                k * unit:(k + 1) * unit, b * LANES:(b + 1) * LANES
+            ]
     pl.semaphore_wait(barrier, len(peers))
 
     pending = []
@@ -70,13 +82,11 @@
             device_id={"fs": (z + 1 if side else z - 1 + n_z) % n_z}, device_id_type=pl.DeviceIdType.MESH,
         )
 
-    send_piece(ORDER[1])
     for side in (0, 1):
         @pl.when((z < n_z - 1) if side else (z > 0))
         def _():
             token_copy(token_ref, z, side).start()
-    for d in ORDER[2:]:
-        send_piece(d)
+    send_piece(ORDER[1])
 
     def zs_of(i):
         return (z - ORDER[i] + n_z) % n_z
@@ -131,37 +141,40 @@
                 else:
                     acc[tt] += value
 
-    def tokens_on():
-        for k in range(1, n_z):
-            for side in (0, 1):
-                here = (z - k >= 0) if side else (z + k < n_z)
-
-                @pl.when(here)
+    def tokens_on(k):
+        for side in (0, 1):
+            here = (z - k >= 0) if side else (z + k < n_z)
+
+            @pl.when(here)
+            def _():
+                slot = (z - k if side else z + k) % n_z
+                token_copy(toks.at[slot], slot, side).wait_recv()
+
+                @pl.when((z + 1 < n_z) if side else (z > 0))
                 def _():
-                    slot = (z - k if side else z + k) % n_z
-                    token_copy(toks.at[slot], slot, side).wait_recv()
-
-                    @pl.when((z + 1 < n_z) if side else (z > 0))
-                    def _():
-                        token_copy(toks.at[slot], slot, side).start()
+                    token_copy(toks.at[slot], slot, side).start()
 
     first(0)
     own_tok.wait()
+    tokens_on(1)
+    send_piece(ORDER[2])
+    second(0)
     first(1)
-    second(0)
-    tokens_on()
-    first(2)
+    tokens_on(2)
+    send_piece(ORDER[3])
     third(0)
     second(1)
+    first(2)
+    third(1)
+    tokens_on(3)
     siblings(0)
     multiply(0)
+    second(2)
     first(3)
-    third(1)
-    second(2)
     siblings(1)
     multiply(1)
+    third(2)
     second(3)
-    third(2)
     siblings(2)
     multiply(2)
     third(3)
@@ -244,27 +257,23 @@
         rows * lax.rsqrt(jnp.mean(rows * rows, axis=-1, keepdims=True) + EPS) * pre_gain
     ).astype(jnp.bfloat16)
 
-    def pieces_of(weight, scale):
-        mine = lax.dynamic_slice_in_dim(weight, y * half, half, 0)
-        low = (mine * scale).astype(jnp.bfloat16).reshape(half, n_z, unit)
-        low = jnp.pad(low, ((0, 0), (0, 0), (0, block - unit)))
-        return low.reshape(half, n_z, block // LANES, LANES).transpose(1, 2, 0, 3).reshape(n_z, -1, LANES)
-
-    mine = lax.dynamic_slice_in_dim(down_weight, y * half, half, 1).astype(jnp.bfloat16)
-    low = mine.reshape(n_z, unit, half // LANES, LANES).transpose(0, 2, 1, 3).reshape(n_z, -1, LANES)
-    pieces = jnp.concatenate(
-        [pieces_of(gate_weight, gate_scale), pieces_of(up_weight, up_scale), low], axis=1
-    )
-    depth = pieces.shape[1]
+    def half_of(weight, axis):
+        return lax.dynamic_slice_in_dim(weight, y * half, half, axis)
+
+    gate_low = (half_of(gate_weight, 0) * gate_scale).astype(jnp.bfloat16)
+    up_low = (half_of(up_weight, 0) * up_scale).astype(jnp.bfloat16)
+    down_low = half_of(down_weight, 1).astype(jnp.bfloat16)
+    depth = (2 * block * half + unit * half) // LANES
     bf16, f32, dma = jnp.bfloat16, jnp.float32, pltpu.SemaphoreType.DMA
     slots = (n_y, n_z, n_t)
     vmem = pl.BlockSpec(memory_space=pltpu.VMEM)
     out = pl.pallas_call(
         functools.partial(fused, (unit, block, half, width)),
         out_shape=jax.ShapeDtypeStruct((n_t, share, width), bf16),
-        in_specs=[vmem] * 4,
+        in_specs=[vmem] * 6,
         out_specs=vmem,
         scratch_shapes=[
+            pltpu.VMEM((n_z, depth, LANES), bf16),
             pltpu.VMEM(slots + (depth, LANES), bf16),
             pltpu.VMEM((n_z, share, width), bf16),
             pltpu.VMEM((n_t, n_z * share, 2 * block), f32),
@@ -277,7 +286,7 @@
         compiler_params=pltpu.CompilerParams(
             collective_id=0, has_side_effects=True, vmem_limit_bytes=60 * 2**20
         ),
-    )(pieces, normed, down_scale[None], post_gain[None])
+    )(gate_low, up_low, down_low, normed, down_scale[None], post_gain[None])
     return out.reshape(n_t * share, width)
 
 

time: 233 us -> 208 us (0.89)
  local copies, waits for them, and re-layouts: 24 us -> 4.14 us
  other arithmetic: 9.41 us -> 6.64 us
    unnamed x11 -> x9, local copies, waits for them, and re-layouts: 9.03 us -> 3.17 us
    transpose x2 -> x0, local copies, waits for them, and re-layouts: 4.61 us -> none  [pieces_of(): low.reshape(half, n_z, block // LANES, LANES).transpose(1, 2, 0, 3)]
    reshape x2 -> x0, local copies, waits for them, and re-layouts: 3.81 us -> none  [quad_body(): mine.reshape(n_z, unit, half // LANES, LANES).transpose(0, 2, 1, 3)]
    dynamic_slice x1 -> x0, local copies, waits for them, and re-layouts: 3.74 us -> none  [pieces_of(): mine = lax.dynamic_slice_in_dim(weight, y * half, half, 0)]
    concatenate x1 -> x0, other arithmetic: 2.92 us -> none  [quad_body(): jnp.concatenate([pieces_of(gate_weight, gate_scale), pieces_of(up_weight,...]
where the time goes in v3:
time: 208 us; the launch traced here: 207 us
  Pallas kernels  197 us (95%)
  other arithmetic  6.64 us (3%)
  local copies, waits for them, and re-layouts  4.14 us (2%)
    pallas_call x1, Pallas kernels, quad_body(): pl.pallas_call(functools.partial(fused, (unit, block, half, width)), out_...  197 us

profile of v3, /device:TPU:0, one launch (start us, length us, event | category | flops | bytes accessed | tf_op | source)
XLA Modules:
  0.0 207.4 jit_solution(11441029031838219608)
XLA Ops:
  0.0 0.0 copy-start
  0.0 0.0 copy-start.2
  0.0 0.0 copy-start.3
  0.0 0.0 copy-start.1
  0.0 1.4 fusion
  1.4 2.5 %fusion.2.token_ref = bf16[128,2048]{1,0:T(8,128)(2,1)} fusion(f32[2048]{0:T(1024)} %param.10, f32[128]{0:T(128)S(1)} %add_rsqrt_fusion, bf16[512,2048]{1,0:T(8,128)(2,1)} %param.9, s32[]{:T(128)S(6)} %select_n.9), kind=kLoop, calls=%fused_computation.7 | loop fusion | flops 1048576 | bytes 1057284 | tf_op jit(solution)/shard_map/convert_element_type | solution.py:258
  3.9 0.0 copy-done
  3.9 1.0 dynamic-slice_convert_fusion.down_ref
  4.9 0.0 copy-done.2
  4.9 0.0 copy-done.3
  4.9 0.0 copy-done.1
  4.9 2.7 %multiply_convert_fusion = (bf16[256,1408]{1,0:T(8,128)(2,1)}, bf16[256,1408]{1,0:T(8,128)(2,1)}) fusion(f32[512,1408]{1,0:T(8,128)S(1)} %copy-done.1, s32[]{:T(128)S(6)} %select_n.8, f32[1408]{0:T(1024)S(1)} %copy-done.2, f32[1408]{0:T(1024)S(1)} %copy-done.3, f32[512,1408]{1,0:T(8,128)} %param.11), kind=kLoop, calls=%fused_computation.1 | loop fusion | flops 1441792 | bytes 4336644 | tf_op jit(solution)/shard_map/convert_element_type | solution.py:264
  7.6 196.6 %shard_map.91 = bf16[4,128,2048]{2,1,0:T(8,128)(2,1)} custom-call(bf16[256,1408]{1,0:T(8,128)(2,1)} %get-tuple-element.6.gate_ref, bf16[256,1408]{1,0:T(8,128)(2,1)} %get-tuple-element.5.up_ref, bf16[1408,256]{1,0:T(8,128)(2,1)} %dynamic-slice_convert_fusion.down_ref, bf16[128,2048]{1,0:T(8,128)(2,1)} %fusion.2.token_ref, f32[1,2048]{1,0:T(1,128)} %bitcast.4, ...), custom_call_target="tpu_custom_call" | custom-call | tf_op jit(solution)/shard_map/pallas_call | solution.py:270
  204.2 3.2 %copy.11 = bf16[512,2048]{1,0:T(8,128)(2,1)} copy(bf16[512,2048]{1,0:T(8,128)(2,1)} %bitcast.3) | data formatting | bytes 4194304
  (1 shorter events, 0.0 us)
Async XLA Ops:
  0.0 3.9 %copy-start = (f32[1408,512]{1,0:T(8,128)S(1)}, f32[1408,512]{1,0:T(8,128)}, u32[]{:S(2)}) copy-start(f32[1408,512]{1,0:T(8,128)} %param.15) | copy-start | bytes 8650756
  0.0 4.9 %copy-start.2 = (f32[1408]{0:T(1024)S(1)}, f32[1408]{0:T(1024)}, u32[]{:S(2)}) copy-start(f32[1408]{0:T(1024)} %param.14) | copy-start | bytes 16900
  0.0 4.9 %copy-start.3 = (f32[1408]{0:T(1024)S(1)}, f32[1408]{0:T(1024)}, u32[]{:S(2)}) copy-start(f32[1408]{0:T(1024)} %param.12) | copy-start | bytes 16900
  0.0 4.9 %copy-start.1 = (f32[512,1408]{1,0:T(8,128)S(1)}, f32[512,1408]{1,0:T(8,128)}, u32[]{:S(2)}) copy-start(f32[512,1408]{1,0:T(8,128)} %param.13) | copy-start | bytes 8650756
